TPU v7x, 32 devices: a whole 2x2x4 slice. The times are simulated.
32 devices in a mesh: rep: 2 (over x), fs: 8 (over z, y), tp: 2 (over core).
Axes of the slice: x: 2, y: 2, z: 4, core: 2. Of those that a mesh axis runs over, the one named last changes fastest.
Arguments:
- activations: bfloat16 [16384, 1024], P(('rep', 'fs', 'tp')), may hold values from -8 to 8
- mixer_gain: float32 [1024], replicated, may hold values from 0.1 to 1.9
- query_weight: bfloat16 [1024, 256], P('fs', 'tp'), may hold values from -0.1875 to 0.1875
- key_weight: bfloat16 [1024, 256], P('fs', 'tp'), may hold values from -0.1875 to 0.1875
- value_weight: bfloat16 [1024, 512], P('fs', 'tp'), may hold values from -0.1875 to 0.1875
- rank_weight: bfloat16 [1024, 16], replicated, may hold values from -0.1875 to 0.1875
- decay_gate_weight: bfloat16 [16, 256], P(None, 'tp'), may hold values from -1.5 to 1.5
- decay_gate_bias: float32 [256], P('tp'), may hold values from -1.5 to 8
- head_gain: float32 [256], replicated, may hold values from 0.1 to 1.9
- output_weight: bfloat16 [512, 1024], P('tp', 'fs'), may hold values from -0.25 to 0.25
- ffn_gain: float32 [1024], replicated, may hold values from 0.1 to 1.9
- gate_weight: bfloat16 [1024, 2816], P('fs', 'tp'), may hold values from -0.1875 to 0.1875
- up_weight: bfloat16 [1024, 2816], P('fs', 'tp'), may hold values from -0.1875 to 0.1875
- down_weight: bfloat16 [2816, 1024], P('tp', 'fs'), may hold values from -0.109375 to 0.109375
Outputs:
- result: bfloat16 [16384, 1024], P(('rep', 'fs', 'tp'))
All inputs are finite; a program needn't handle non-finite values.
Results may differ from a plain program's by a relative error of at most 0.0056.
Values may be sent and summed in bfloat16 or wider, within the bound.
No kernel may reach another device: no remote copies, remote signals or barrier semaphores. Data moves between devices by JAX's collectives and lax.ppermute only.
A program may use at most 64 MiB of HBM per device.

v0:
```python
import jax
import jax.numpy as jnp
from jax import lax
from jax.sharding import PartitionSpec as P

DK = 128
DV = 256
BLOCK = 64
epsilon = 1e-06
decay_softness = 16.0
highest = lax.Precision.HIGHEST


def rms_scale(values, gains):
    return values * lax.rsqrt(jnp.mean(values * values, axis=-1, keepdims=True) + epsilon) * gains


def linear_attention(queries, keys_all, values_all, decay_logarithm, head_count):
    length = queries.shape[0]
    number = length // BLOCK
    halfway = BLOCK // 2
    causal = jnp.tril(jnp.ones((BLOCK, BLOCK), bool))

    def to_blocks(matrix):
        return matrix.astype(jnp.float32).reshape(
            number, BLOCK, head_count, matrix.shape[1] // head_count
        )

    block_query = to_blocks(queries)
    block_key = to_blocks(keys_all)
    block_value = to_blocks(values_all)
    cumulative = jnp.cumsum(to_blocks(decay_logarithm), axis=1)
    middle = cumulative[:, halfway - 1 : halfway]
    query_local = block_query * jnp.exp(cumulative - middle)
    key_local = block_key * jnp.exp(middle - cumulative)
    scores = jnp.einsum("nthd,nshd->nhts", query_local, key_local, precision=highest)
    scores = jnp.where(causal[None, None], scores, 0.0)
    within = jnp.einsum("nhts,nshv->nthv", scores, block_value, precision=highest)
    lasting = cumulative[:, -1]
    update = jnp.einsum(
        "nshd,nshv->nhdv",
        block_key * jnp.exp(lasting[:, None] - cumulative),
        block_value,
        precision=highest,
    )

    def advance(memory, inputs):
        fade, addition = inputs
        return (jnp.exp(fade)[:, :, None] * memory + addition, memory)

    key_width = queries.shape[1] // head_count
    value_width = values_all.shape[1] // head_count
    initial = jnp.zeros((head_count, key_width, value_width), jnp.float32)
    earlier = lax.scan(advance, initial, (lasting, update))[1]
    carried = jnp.einsum(
        "nthd,nhdv->nthv", block_query * jnp.exp(cumulative), earlier, precision=highest
    )
    return (within + carried).reshape(length, head_count, value_width)


def project_inputs(source, weight):
    return jnp.dot(source, weight, preferred_element_type=jnp.float32)


def local(
    activations,
    mixer_gain,
    query_weight,
    key_weight,
    value_weight,
    rank_weight,
    decay_gate_weight,
    decay_gate_bias,
    head_gain,
    output_weight,
    ffn_gain,
    gate_weight,
    up_weight,
    down_weight,
):
    residual = activations.astype(jnp.float32)
    normed = rms_scale(residual, mixer_gain).astype(jnp.bfloat16)
    rank_slice = project_inputs(normed, rank_weight).astype(jnp.bfloat16)
    sequence, rank_slices_gathered = (
        lax.all_gather(normed, "tp", axis=0, tiled=True),
        lax.all_gather(rank_slice, "tp", axis=0, tiled=True),
    )
    length = sequence.shape[0]
    query_full, key_full, value_full = (
        lax.all_gather(query_weight, "fs", axis=0, tiled=True),
        lax.all_gather(key_weight, "fs", axis=0, tiled=True),
        lax.all_gather(value_weight, "fs", axis=0, tiled=True),
    )
    queries = project_inputs(sequence, query_full).astype(jnp.bfloat16)
    keys_all = project_inputs(sequence, key_full).astype(jnp.bfloat16)
    values_all = project_inputs(sequence, value_full).astype(jnp.bfloat16)
    decay_logarithm = (
        jax.nn.log_sigmoid(
            project_inputs(rank_slices_gathered, decay_gate_weight) + decay_gate_bias
        )
        / decay_softness
    )
    head_count = query_weight.shape[1] // DK
    attended = linear_attention(queries, keys_all, values_all, decay_logarithm, head_count)
    head_rows = rms_scale(attended, head_gain).astype(jnp.bfloat16).reshape(length, head_count * DV)
    own_rows = lax.all_to_all(head_rows, "tp", split_axis=0, concat_axis=1, tiled=True)
    tall_out = lax.all_gather(output_weight, "tp", axis=0, tiled=True)
    whole_out = lax.all_gather(tall_out, "fs", axis=1, tiled=True)
    mixed = residual + project_inputs(own_rows, whole_out)
    ffn_normed = rms_scale(mixed, ffn_gain).astype(jnp.bfloat16)
    ffn_sequence = lax.all_gather(ffn_normed, "tp", axis=0, tiled=True)
    gate_full, up_full = (
        lax.all_gather(gate_weight, "fs", axis=0, tiled=True),
        lax.all_gather(up_weight, "fs", axis=0, tiled=True),
    )
    down_full = lax.all_gather(down_weight, "fs", axis=1, tiled=True)
    hidden = (
        jax.nn.silu(project_inputs(ffn_sequence, gate_full)) * project_inputs(ffn_sequence, up_full)
    ).astype(jnp.bfloat16)
    result = mixed + lax.psum_scatter(
        project_inputs(hidden, down_full).astype(jnp.bfloat16),
        "tp",
        scatter_dimension=0,
        tiled=True,
    ).astype(jnp.float32)
    return result.astype(jnp.bfloat16)


def solution(mesh):
    in_specs = (
        P(("rep", "fs", "tp"), None),
        P(),
        P("fs", "tp"),
        P("fs", "tp"),
        P("fs", "tp"),
        P(),
        P(None, "tp"),
        P("tp"),
        P(),
        P("tp", "fs"),
        P(),
        P("fs", "tp"),
        P("fs", "tp"),
        P("tp", "fs"),
    )
    out_specs = P(("rep", "fs", "tp"), None)
    return jax.shard_map(local, mesh=mesh, in_specs=in_specs, out_specs=out_specs, check_vma=False)
```

profile of v0, /device:TPU:0, one launch (start us, length us, event | category | flops | bytes accessed | tf_op | source)
XLA Modules:
  0.0 369.9 jit_solution(17549334003282702146)
XLA Ops:
  6.5 1.5 fusion.2
  8.1 2.5 fusion.4
  10.7 2.2 all_gather.38
  13.0 1.6 convolution_convert_fusion.3
  14.6 2.1 all_gather.36
  17.6 32.6 %all_gather.37 = bf16[1024,128]{1,0:T(8,128)(2,1)S(1)} all-gather(bf16[128,128]{1,0:T(8,128)(2,1)S(1)} %copy-done.8), channel_id=1, replica_groups=mesh['rep'=2,'fs'=8,'tp'=2] {'fs'}, dimensions={0}, use_global_device_ids=true | all-gather | bytes 294912 | tf_op jit(solution)/shard_map/all_gather | solution.py:91
  50.2 31.1 %all_gather.35 = bf16[1024,128]{1,0:T(8,128)(2,1)S(1)} all-gather(bf16[128,128]{1,0:T(8,128)(2,1)S(1)} %copy-done.9), channel_id=1, replica_groups=mesh['rep'=2,'fs'=8,'tp'=2] {'fs'}, dimensions={0}, use_global_device_ids=true | all-gather | bytes 294912 | tf_op jit(solution)/shard_map/all_gather | solution.py:90
  81.3 31.3 %all_gather.34 = bf16[1024,256]{1,0:T(8,128)(2,1)S(1)} all-gather(bf16[128,256]{1,0:T(8,128)(2,1)S(1)} %copy-done.7), channel_id=1, replica_groups=mesh['rep'=2,'fs'=8,'tp'=2] {'fs'}, dimensions={0}, use_global_device_ids=true | all-gather | bytes 589824 | tf_op jit(solution)/shard_map/all_gather | solution.py:92
  112.6 2.4 convolution_convert_fusion.1
  115.8 1.6 fusion.14
  119.2 12.6 %while.13 = (s32[]{:T(128)}, f32[1,128,256]{2,1,0:T(8,128)S(1)}, f32[16,1,128,256]{3,2,1,0:T(8,128)}, f32[16,1,128]{2,1,0:T(1,128)S(1)}, f32[16,1,128,256]{3,2,1,0:T(8,128)S(1)}, /*index=5*/s32[]{:T(128)}, s32[]{:T(128)}) while((s32[]{:T(128)}, f32[1,128,256]{2,1,0:T(8,128)S(1)}, f32[16,1,128,256]{3,2,1,0:T(8,128)}, ...), condition=%wide.region_3.4_spmd.clone, body=%wide.region_2.3_spmd.clone.sunk | while | flops 131075 | bytes 657504 | solution.py:54
  131.8 2.2 convolution_select_fusion
  134.1 3.0 fusion.5
  139.2 3.5 all-to-all-start
  142.8 1.7 all-to-all-done
  145.2 2.2 multiply_reduce_fusion
  150.7 10.0 %all-gather.11.cloned.1.call-done = bf16[1024,1024]{1,0:T(8,128)(2,1)} async-done(((bf16[512,1024]{1,0:T(8,128)(2,1)}), bf16[1024,1024]{1,0:T(8,128)(2,1)}) %all-gather.11.cloned.1.call-update) | async-done | bytes 2097168 | tf_op jit(solution)/shard_map/all_gather | solution.py:111
  160.7 60.5 %all-gather.13.cloned.1.call-done = bf16[1024,1408]{1,0:T(8,128)(2,1)} async-done(((bf16[128,1408]{1,0:T(8,128)(2,1)}), bf16[1024,1408]{1,0:T(8,128)(2,1)}) %all-gather.13.cloned.1.call-update) | async-done | bytes 2883600 | tf_op jit(solution)/shard_map/all_gather | solution.py:113
  221.2 8.3 %fusion.27 = f32[1024,1408]{1,0:T(8,128)} fusion(bf16[1024,1024]{1,0:T(8,128)(2,1)} %all-gather.11.cloned.1.call-done, bf16[1024,1408]{1,0:T(8,128)(2,1)} %all-gather.13.cloned.1.call-done), kind=kOutput, calls=%fused_computation.58 | convolution fusion | flops 2952790016 | bytes 10747904 | tf_op jit(solution)/shard_map/dot_general | solution.py:62
  229.6 49.6 %all-gather.15.cloned.1.call-done = bf16[1024,1408]{1,0:T(8,128)(2,1)} async-done(((bf16[128,1408]{1,0:T(8,128)(2,1)}), bf16[1024,1408]{1,0:T(8,128)(2,1)}) %all-gather.15.cloned.1.call-update) | async-done | bytes 2883600 | tf_op jit(solution)/shard_map/all_gather | solution.py:114
  279.2 60.1 %all-gather.17.cloned.1.call-done = bf16[1408,1024]{1,0:T(8,128)(2,1)} async-done(((bf16[1408,128]{1,0:T(8,128)(2,1)}), bf16[1408,1024]{1,0:T(8,128)(2,1)}) %all-gather.17.cloned.1.call-update) | async-done | bytes 2883600 | tf_op jit(solution)/shard_map/all_gather | solution.py:116
  339.3 13.1 %fusion.8 = bf16[1024,1024]{1,0:T(8,128)(2,1)} fusion(bf16[1408,1024]{1,0:T(8,128)(2,1)} %all-gather.17.cloned.1.call-done, f32[1024,1408]{1,0:T(8,128)} %fusion.27, bf16[1024,1024]{1,0:T(8,128)(2,1)} %all-gather.11.cloned.1.call-done, bf16[1024,1408]{1,0:T(8,128)(2,1)} %all-gather.15.cloned.1.call-done), kind=kOutput, calls=%fused_computation.18 | convolution fusion | flops 5915279360 | bytes 15728640 | tf_op jit(solution)/shard_map/dot_general | solution.py:62
  352.4 8.1 %reduce-scatter.2.cloned.1.call-done = bf16[512,1024]{1,0:T(8,128)(2,1)} async-done(((bf16[1024,1024]{1,0:T(8,128)(2,1)}), bf16[512,1024]{1,0:T(8,128)(2,1)}) %reduce-scatter.2.cloned.1.call-update) | async-done | bytes 1048592 | tf_op jit(solution)/shard_map/reduce_scatter | solution.py:120
  360.5 2.5 add_convert_fusion
  (111 shorter events, 21.8 us)
Async XLA Ops:
  6.5 6.4 %copy-start = (bf16[1024,16]{0,1:T(8,128)(2,1)S(1)}, bf16[1024,16]{0,1:T(8,128)(2,1)}, u32[]{:S(2)}) copy-start(bf16[1024,16]{0,1:T(8,128)(2,1)} %param.21) | copy-start | bytes 98308
  6.5 106.0 %all-gather.7.cloned.1.call-start = ((), (), s32[]{:S(2)}) async-start(), calls=%async_computation.2 | async-start | bytes 3145728 | tf_op jit(solution)/shard_map/all_gather | solution.py:85
  6.5 4.2 %copy-start.6 = (bf16[256,128]{1,0:T(8,128)(2,1)S(1)}, bf16[256,128]{1,0:T(8,128)(2,1)}, u32[]{:S(2)}) copy-start(bf16[256,128]{1,0:T(8,128)(2,1)} %param.25) | copy-start | bytes 196612
  8.1 8.7 %copy-start.12 = (bf16[16,128]{1,0:T(8,128)(2,1)S(1)}, bf16[16,128]{1,0:T(8,128)(2,1)}, u32[]{:S(2)}) copy-start(bf16[16,128]{1,0:T(8,128)(2,1)} %param.22) | copy-start | bytes 12292
  8.1 8.7 %copy-start.13 = (f32[128]{0:T(128)S(1)}, f32[128]{0:T(128)}, u32[]{:S(2)}) copy-start(f32[128]{0:T(128)} %param.23) | copy-start | bytes 1540
  10.7 132.1 %all-gather.9.cloned.1.call-start = ((), (), s32[]{:S(2)}) async-start(), calls=%async_computation.3 | async-start | bytes 1179648 | tf_op jit(solution)/shard_map/all_gather | solution.py:108
  13.0 4.6 %copy-start.8 = (bf16[128,128]{1,0:T(8,128)(2,1)S(1)}, bf16[128,128]{1,0:T(8,128)(2,1)}, u32[]{:S(2)}) copy-start(bf16[128,128]{1,0:T(8,128)(2,1)} %param.19) | copy-start | bytes 98308
  14.6 35.6 %copy-start.9 = (bf16[128,128]{1,0:T(8,128)(2,1)S(1)}, bf16[128,128]{1,0:T(8,128)(2,1)}, u32[]{:S(2)}) copy-start(bf16[128,128]{1,0:T(8,128)(2,1)} %param.18) | copy-start | bytes 98308
  14.6 66.6 %copy-start.7 = (bf16[128,256]{1,0:T(8,128)(2,1)S(1)}, bf16[128,256]{1,0:T(8,128)(2,1)}, u32[]{:S(2)}) copy-start(bf16[128,256]{1,0:T(8,128)(2,1)} %param.20) | copy-start | bytes 196612
  112.6 2.5 copy-start.2
  118.1 1.1 copy-start.4
  134.0 3.0 copy-start.5
  137.1 1.2 copy-start.11
  137.8 7.4 %copy-start.1 = (bf16[512,1024]{1,0:T(8,128)(2,1)S(1)}, bf16[512,1024]{1,0:T(8,128)(2,1)}, u32[]{:S(2)}) copy-start(bf16[512,1024]{1,0:T(8,128)(2,1)} %param.16) | copy-start | bytes 3145732
  139.2 5.2 %all-to-all-start = ((bf16[2,512,256]{1,2,0:T(8,128)(2,1)}), bf16[2,512,256]{1,2,0:T(8,128)(2,1)S(1)}, u32[]{:S(2)}, u32[]{:S(2)}) async-start(bf16[2,512,256]{1,2,0:T(8,128)(2,1)} %multiply_convert_fusion.2), calls=%async_computation | async-start | bytes 1048576 | tf_op jit(solution)/shard_map/all_to_all | solution.py:106
  142.7 18.0 %all-gather.11.cloned.1.call-start = ((), (), s32[]{:S(2)}) async-start(), calls=%async_computation.4 | async-start | bytes 3145728 | tf_op jit(solution)/shard_map/all_gather | solution.py:111
  144.4 0.8 copy-start.3
  145.2 2.2 copy-start.10
  148.7 72.5 %all-gather.13.cloned.1.call-start = ((), (), s32[]{:S(2)}) async-start(), calls=%async_computation.5 | async-start | bytes 3244032 | tf_op jit(solution)/shard_map/all_gather | solution.py:113
  149.3 129.9 %all-gather.15.cloned.1.call-start = ((), (), s32[]{:S(2)}) async-start(), calls=%async_computation.6 | async-start | bytes 3244032 | tf_op jit(solution)/shard_map/all_gather | solution.py:114
  149.9 189.5 %all-gather.17.cloned.1.call-start = ((), (), s32[]{:S(2)}) async-start(), calls=%async_computation.7 | async-start | bytes 3244032 | tf_op jit(solution)/shard_map/all_gather | solution.py:116
  150.4 210.1 %reduce-scatter.2.cloned.1.call-start = ((), (), s32[]{:S(2)}) async-start(), calls=%async_computation.8 | async-start | bytes 3145728 | tf_op jit(solution)/shard_map/reduce_scatter | solution.py:120
Sparse Core Ops, SparseCore 0:
  10.8 13.2 all-gather.6
  26.1 42.2 all-gather.8
  148.8 11.8 all-gather.10
  162.7 58.4 all-gather.12
  223.3 55.9 all-gather.14
  281.1 58.1 all-gather.16
  352.5 7.9 reduce-scatter.1
where the time goes:
time: 370 us
  waiting for transfers between devices  192 us (52%)
  blocking collectives  99.3 us (27%)
  matrix products  36.6 us (10%)
  other arithmetic  22.9 us (6%)
  between operations  13.8 us (4%)
  starting transfers between devices  3.91 us (1%)
    all_gather x1, waiting for transfers between devices, local(): lax.all_gather(gate_weight, 'fs', axis=0, tiled=True)  60.5 us
    all_gather x1, waiting for transfers between devices, local(): down_full = lax.all_gather(down_weight, 'fs', axis=1, tiled=True)  60.1 us
    all_gather x1, waiting for transfers between devices, local(): lax.all_gather(up_weight, 'fs', axis=0, tiled=True)  49.6 us
    all_gather x1, blocking collectives, local(): lax.all_gather(key_weight, 'fs', axis=0, tiled=True)  32.6 us
    all_gather x1, blocking collectives, local(): lax.all_gather(value_weight, 'fs', axis=0, tiled=True)  31.3 us
    all_gather x1, blocking collectives, local(): lax.all_gather(query_weight, 'fs', axis=0, tiled=True)  31.1 us
    dot_general x8, matrix products, project_inputs(): return jnp.dot(source, weight, preferred_element_type=jnp.float32)  29.6 us
    dynamic_update_slice x16, other arithmetic, linear_attention(): earlier = lax.scan(advance, initial, (lasting, update))[1]  10.6 us
  transfers between devices with their start and end apart: 8, of which 6 were waited for; matrix products, arithmetic and copies ran while one was open for 10% of the time, Pallas kernels for 0%

commit v1 on v0

--- a/solution.py
+++ b/solution.py
@@ -113,7 +113,7 @@
         lax.all_gather(gate_weight, "fs", axis=0, tiled=True),
         lax.all_gather(up_weight, "fs", axis=0, tiled=True),
     )
-    down_full = lax.all_gather(down_weight, "fs", axis=1, tiled=True)
+    down_full = jnp.concatenate(lax.all_gather(down_weight, "fs"), axis=1)
     hidden = (
         jax.nn.silu(project_inputs(ffn_sequence, gate_full)) * project_inputs(ffn_sequence, up_full)
     ).astype(jnp.bfloat16)

time: 370 us -> 313 us (0.85)
  waiting for transfers between devices: 192 us -> 129 us
  local copies, waits for them, and re-layouts: 1.33 us -> 5.89 us
    all_gather x1, waiting for transfers between devices: 60.1 us -> 0.02 us  [local(): down_full = jnp.concatenate(lax.all_gather(down_weight, 'fs'), axis=1)]
    reshape x0 -> x1, local copies, waits for them, and re-layouts: none -> 4.56 us  [local(): down_full = jnp.concatenate(lax.all_gather(down_weight, 'fs'), axis=1)]
  transfers between devices with their start and end apart: 8 -> 8, of which waited for: 6 -> 5; matrix products, arithmetic and copies ran while one was open for 10% -> 14% of each run, Pallas kernels for 0% -> 0%
where the time goes in v1:
time: 313 us
  waiting for transfers between devices  129 us (41%)
  blocking collectives  101 us (32%)
  matrix products  36.7 us (12%)
  other arithmetic  22.9 us (7%)
  between operations  13.8 us (4%)
  local copies, waits for them, and re-layouts  5.89 us (2%)
  starting transfers between devices  3.92 us (1%)
    all_gather x1, waiting for transfers between devices, local(): lax.all_gather(gate_weight, 'fs', axis=0, tiled=True)  60.5 us
    all_gather x1, waiting for transfers between devices, local(): lax.all_gather(up_weight, 'fs', axis=0, tiled=True)  49.7 us
    all_gather x1, blocking collectives, local(): lax.all_gather(value_weight, 'fs', axis=0, tiled=True)  32.9 us
    all_gather x1, blocking collectives, local(): lax.all_gather(key_weight, 'fs', axis=0, tiled=True)  32.5 us
    all_gather x1, blocking collectives, local(): lax.all_gather(query_weight, 'fs', axis=0, tiled=True)  31.3 us
    dot_general x8, matrix products, project_inputs(): return jnp.dot(source, weight, preferred_element_type=jnp.float32)  29.6 us
    dynamic_update_slice x16, other arithmetic, linear_attention(): earlier = lax.scan(advance, initial, (lasting, update))[1]  10.6 us
    reduce_scatter x1, waiting for transfers between devices, local(): lax.psum_scatter(project_inputs(hidden, down_full).astype(jnp.bfloat16),...  8.51 us
  transfers between devices with their start and end apart: 8, of which 5 were waited for; matrix products, arithmetic and copies ran while one was open for 14% of the time, Pallas kernels for 0%

profile of v1, /device:TPU:0, one launch (start us, length us, event | category | flops | bytes accessed | tf_op | source)
XLA Modules:
  0.0 312.8 jit_solution(3237864823844066380)
XLA Ops:
  6.5 1.5 fusion.2
  8.1 2.5 fusion.4
  10.7 2.2 all_gather.41
  13.7 1.6 convolution_convert_fusion.3
  15.4 1.8 all_gather.39
  18.1 32.5 %all_gather.40 = bf16[1024,128]{1,0:T(8,128)(2,1)S(1)} all-gather(bf16[128,128]{1,0:T(8,128)(2,1)S(1)} %copy-done.8), channel_id=1, replica_groups=mesh['rep'=2,'fs'=8,'tp'=2] {'fs'}, dimensions={0}, use_global_device_ids=true | all-gather | bytes 294912 | tf_op jit(solution)/shard_map/all_gather | solution.py:91
  50.5 31.3 %all_gather.38 = bf16[1024,128]{1,0:T(8,128)(2,1)S(1)} all-gather(bf16[128,128]{1,0:T(8,128)(2,1)S(1)} %copy-done.9), channel_id=1, replica_groups=mesh['rep'=2,'fs'=8,'tp'=2] {'fs'}, dimensions={0}, use_global_device_ids=true | all-gather | bytes 294912 | tf_op jit(solution)/shard_map/all_gather | solution.py:90
  81.8 32.9 %all_gather.37 = bf16[1024,256]{1,0:T(8,128)(2,1)S(1)} all-gather(bf16[128,256]{1,0:T(8,128)(2,1)S(1)} %copy-done.7), channel_id=1, replica_groups=mesh['rep'=2,'fs'=8,'tp'=2] {'fs'}, dimensions={0}, use_global_device_ids=true | all-gather | bytes 589824 | tf_op jit(solution)/shard_map/all_gather | solution.py:92
  114.7 2.4 convolution_convert_fusion.1
  118.0 1.6 fusion.14
  121.4 12.6 %while.13 = (s32[]{:T(128)}, f32[1,128,256]{2,1,0:T(8,128)S(1)}, f32[16,1,128,256]{3,2,1,0:T(8,128)}, f32[16,1,128]{2,1,0:T(1,128)S(1)}, f32[16,1,128,256]{3,2,1,0:T(8,128)S(1)}, /*index=5*/s32[]{:T(128)}, s32[]{:T(128)}) while((s32[]{:T(128)}, f32[1,128,256]{2,1,0:T(8,128)S(1)}, f32[16,1,128,256]{3,2,1,0:T(8,128)}, ...), condition=%wide.region_3.4_spmd.clone, body=%wide.region_2.3_spmd.clone.sunk | while | flops 131075 | bytes 657504 | solution.py:54
  134.0 2.2 convolution_select_fusion
  136.3 3.0 fusion.5
  141.4 3.5 %all-to-all-start = ((bf16[2,512,256]{1,2,0:T(8,128)(2,1)}), bf16[2,512,256]{1,2,0:T(8,128)(2,1)S(1)}, u32[]{:S(2)}, u32[]{:S(2)}) async-start(bf16[2,512,256]{1,2,0:T(8,128)(2,1)} %multiply_convert_fusion.2), calls=%async_computation | async-start | bytes 1048576 | tf_op jit(solution)/shard_map/all_to_all | solution.py:106
  145.0 1.7 all-to-all-done
  147.4 2.2 multiply_reduce_fusion
  152.3 4.6 %copy.46 = bf16[1408,8,128]{0,2,1:T(8,128)(2,1)} copy(bf16[1408,8,128]{2,0,1:T(8,128)(2,1)} %bitcast.87) | data formatting | bytes 5767168 | tf_op jit(solution)/shard_map/reshape | solution.py:116
  156.9 6.4 %all-gather.12.cloned.1.call-done = bf16[1024,1024]{1,0:T(8,128)(2,1)} async-done(((bf16[512,1024]{1,0:T(8,128)(2,1)}), bf16[1024,1024]{1,0:T(8,128)(2,1)}) %all-gather.12.cloned.1.call-update) | async-done | bytes 2097168 | tf_op jit(solution)/shard_map/all_gather | solution.py:111
  163.3 60.5 %all-gather.14.cloned.1.call-done = bf16[1024,1408]{1,0:T(8,128)(2,1)} async-done(((bf16[128,1408]{1,0:T(8,128)(2,1)}), bf16[1024,1408]{1,0:T(8,128)(2,1)}) %all-gather.14.cloned.1.call-update) | async-done | bytes 2883600 | tf_op jit(solution)/shard_map/all_gather | solution.py:113
  223.8 8.3 %fusion.27 = f32[1024,1408]{1,0:T(8,128)} fusion(bf16[1024,1024]{1,0:T(8,128)(2,1)} %all-gather.12.cloned.1.call-done, bf16[1024,1408]{1,0:T(8,128)(2,1)} %all-gather.14.cloned.1.call-done), kind=kOutput, calls=%fused_computation.58 | convolution fusion | flops 2952790016 | bytes 10747904 | tf_op jit(solution)/shard_map/dot_general | solution.py:62
  232.2 49.7 %all-gather.16.cloned.1.call-done = bf16[1024,1408]{1,0:T(8,128)(2,1)} async-done(((bf16[128,1408]{1,0:T(8,128)(2,1)}), bf16[1024,1408]{1,0:T(8,128)(2,1)}) %all-gather.16.cloned.1.call-update) | async-done | bytes 2883600 | tf_op jit(solution)/shard_map/all_gather | solution.py:114
  281.8 13.1 %fusion.8 = bf16[1024,1024]{1,0:T(8,128)(2,1)} fusion(bf16[1408,1024]{0,1:T(8,128)(2,1)} %bitcast.88, f32[1024,1408]{1,0:T(8,128)} %fusion.27, bf16[1024,1024]{1,0:T(8,128)(2,1)} %all-gather.12.cloned.1.call-done, bf16[1024,1408]{1,0:T(8,128)(2,1)} %all-gather.16.cloned.1.call-done), kind=kOutput, calls=%fused_computation.18 | convolution fusion | flops 5915279360 | bytes 15728640 | tf_op jit(solution)/shard_map/dot_general | solution.py:62
  294.9 8.5 %reduce-scatter.2.cloned.1.call-done = bf16[512,1024]{1,0:T(8,128)(2,1)} async-done(((bf16[1024,1024]{1,0:T(8,128)(2,1)}), bf16[512,1024]{1,0:T(8,128)(2,1)}) %reduce-scatter.2.cloned.1.call-update) | async-done | bytes 1048592 | tf_op jit(solution)/shard_map/reduce_scatter | solution.py:120
  303.4 2.5 add_convert_fusion
  (112 shorter events, 22.1 us)
Async XLA Ops:
  6.5 7.2 %copy-start = (bf16[1024,16]{0,1:T(8,128)(2,1)S(1)}, bf16[1024,16]{0,1:T(8,128)(2,1)}, u32[]{:S(2)}) copy-start(bf16[1024,16]{0,1:T(8,128)(2,1)} %param.21) | copy-start | bytes 98308
  6.5 108.2 %all-gather.8.cloned.1.call-start = ((), (), s32[]{:S(2)}) async-start(), calls=%async_computation.2 | async-start | bytes 3145728 | tf_op jit(solution)/shard_map/all_gather | solution.py:85
  6.5 4.2 %copy-start.6 = (bf16[256,128]{1,0:T(8,128)(2,1)S(1)}, bf16[256,128]{1,0:T(8,128)(2,1)}, u32[]{:S(2)}) copy-start(bf16[256,128]{1,0:T(8,128)(2,1)} %param.25) | copy-start | bytes 196612
  8.1 9.1 %copy-start.12 = (bf16[16,128]{1,0:T(8,128)(2,1)S(1)}, bf16[16,128]{1,0:T(8,128)(2,1)}, u32[]{:S(2)}) copy-start(bf16[16,128]{1,0:T(8,128)(2,1)} %param.22) | copy-start | bytes 12292
  8.1 9.1 %copy-start.13 = (f32[128]{0:T(128)S(1)}, f32[128]{0:T(128)}, u32[]{:S(2)}) copy-start(f32[128]{0:T(128)} %param.23) | copy-start | bytes 1540
  10.7 134.3 %all-gather.10.cloned.1.call-start = ((), (), s32[]{:S(2)}) async-start(), calls=%async_computation.3 | async-start | bytes 1179648 | tf_op jit(solution)/shard_map/all_gather | solution.py:108
  12.9 5.1 %copy-start.8 = (bf16[128,128]{1,0:T(8,128)(2,1)S(1)}, bf16[128,128]{1,0:T(8,128)(2,1)}, u32[]{:S(2)}) copy-start(bf16[128,128]{1,0:T(8,128)(2,1)} %param.19) | copy-start | bytes 98308
  12.9 139.4 %all-gather.18.cloned.1.call-start = ((), (), s32[]{:S(2)}) async-start(), calls=%async_computation.8 | async-start | bytes 3244032 | tf_op jit(solution)/shard_map/all_gather | solution.py:116
  13.7 36.9 %copy-start.9 = (bf16[128,128]{1,0:T(8,128)(2,1)S(1)}, bf16[128,128]{1,0:T(8,128)(2,1)}, u32[]{:S(2)}) copy-start(bf16[128,128]{1,0:T(8,128)(2,1)} %param.18) | copy-start | bytes 98308
  13.7 68.1 %copy-start.7 = (bf16[128,256]{1,0:T(8,128)(2,1)S(1)}, bf16[128,256]{1,0:T(8,128)(2,1)}, u32[]{:S(2)}) copy-start(bf16[128,256]{1,0:T(8,128)(2,1)} %param.20) | copy-start | bytes 196612
  114.7 2.5 copy-start.2
  120.3 1.1 copy-start.4
  136.3 3.0 copy-start.5
  139.3 1.2 copy-start.11
  140.0 7.4 %copy-start.1 = (bf16[512,1024]{1,0:T(8,128)(2,1)S(1)}, bf16[512,1024]{1,0:T(8,128)(2,1)}, u32[]{:S(2)}) copy-start(bf16[512,1024]{1,0:T(8,128)(2,1)} %param.16) | copy-start | bytes 3145732
  141.4 5.2 %all-to-all-start = ((bf16[2,512,256]{1,2,0:T(8,128)(2,1)}), bf16[2,512,256]{1,2,0:T(8,128)(2,1)S(1)}, u32[]{:S(2)}, u32[]{:S(2)}) async-start(bf16[2,512,256]{1,2,0:T(8,128)(2,1)} %multiply_convert_fusion.2), calls=%async_computation | async-start | bytes 1048576 | tf_op jit(solution)/shard_map/all_to_all | solution.py:106
  144.9 18.4 %all-gather.12.cloned.1.call-start = ((), (), s32[]{:S(2)}) async-start(), calls=%async_computation.4 | async-start | bytes 3145728 | tf_op jit(solution)/shard_map/all_gather | solution.py:111
  146.6 0.8 copy-start.3
  147.4 2.2 copy-start.10
  150.9 72.9 %all-gather.14.cloned.1.call-start = ((), (), s32[]{:S(2)}) async-start(), calls=%async_computation.5 | async-start | bytes 3244032 | tf_op jit(solution)/shard_map/all_gather | solution.py:113
  151.5 130.3 %all-gather.16.cloned.1.call-start = ((), (), s32[]{:S(2)}) async-start(), calls=%async_computation.6 | async-start | bytes 3244032 | tf_op jit(solution)/shard_map/all_gather | solution.py:114
  152.1 151.3 %reduce-scatter.2.cloned.1.call-start = ((), (), s32[]{:S(2)}) async-start(), calls=%async_computation.7 | async-start | bytes 3145728 | tf_op jit(solution)/shard_map/reduce_scatter | solution.py:120
Sparse Core Ops, SparseCore 0:
  10.8 13.2 all-gather.7
  26.1 42.5 all-gather.9
  70.9 59.4 all-gather.17
  151.0 12.2 all-gather.11
  165.3 58.4 all-gather.13
  225.9 55.9 all-gather.15
  295.0 8.3 reduce-scatter.1
